TPU v7x, 32 devices: a whole 2x2x4 slice. The times are simulated.
32 devices in a mesh: grp: 2 (over y), sp: 4 (over z), tp: 4 (over x, core).
Axes of the slice: x: 2, y: 2, z: 4, core: 2. Of those that a mesh axis runs over, the one named last changes fastest.
Arguments:
- stream: bfloat16 [6144, 4096], P(('grp', 'sp'), 'tp'), parts along dimension 0, may hold values from -400 to 400
- in_weight: bfloat16 [2, 1024, 4096], P(None, 'sp', 'tp'), may hold values from -0.09375 to 0.09375
- out_weight: bfloat16 [2, 1024, 4096], P(None, 'sp', 'tp'), may hold values from -0.1875 to 0.1875
- group_mix: bfloat16 [2, 4, 256, 256], replicated, may hold values from -0.375 to 0.375
- pool_gain: float32 [2, 1024], replicated, may hold values from 0.1 to 1.9
- norm_gain: float32 [2, 4096], P(None, 'tp'), may hold values from 0.1 to 1.9
- norm_shift: float32 [2, 4096], P(None, 'tp'), may hold values from -3 to 3
Outputs:
- refined: bfloat16 [6144, 4096], P(('grp', 'sp'), 'tp'), parts along dimension 0
There are 2 independent parts, one for each index of `grp`. A program takes and returns all parts, laid end to end along the dimension named above; an argument that names none is the same for every part. Nothing has to cross between parts.
All inputs are finite; a program needn't handle non-finite values.
Results may differ from a plain program's by a relative error of at most 0.015.
Values may be sent and summed in bfloat16 or wider, within the bound.
A program may use at most 64 MiB of HBM per device.

v0:
```python
import jax
import jax.numpy as jnp
from jax import lax
from jax.sharding import PartitionSpec as P

D = 4096
POOL = 1024
GROUPS = 4
GROUP_WIDTH = 256
LAYERS = 2
epsilon = 1e-05


def passed_along(block, axis, distance):
    devices = range(lax.axis_size(axis))
    route = [(i - distance, i) for i in devices if i - distance in devices]
    return lax.ppermute(block, axis, route)


def pooled_windows(hidden, tok_start):
    reach = 2**GROUPS - 1
    length = hidden.shape[1]
    channels = hidden.shape[0]
    earlier = passed_along(hidden[:, length - reach :], "sp", 1)
    extended = jnp.concatenate([earlier, hidden], axis=1).astype(jnp.float32)
    group_ids = (jnp.arange(channels, dtype=jnp.int32) // GROUP_WIDTH)[:, None]
    running = extended
    window_sums = jnp.zeros((channels, length), jnp.float32)
    for octave in range(GROUPS):
        offset = 2**octave
        running = running[:, offset:] + running[:, : running.shape[1] - offset]
        window_sums = jnp.where(
            group_ids == octave, running[:, running.shape[1] - length :], window_sums
        )
    positions = (tok_start + jnp.arange(length, dtype=jnp.int32) + 1).astype(jnp.float32)
    widths = jnp.exp2((group_ids + 1).astype(jnp.float32))
    counts = jnp.minimum(positions[None, :], widths)
    return (window_sums / counts - hidden.astype(jnp.float32)).astype(jnp.bfloat16)


def per_device(stream, in_weight, out_weight, group_mix, pool_gain, norm_gain, norm_shift):
    tok_rows = stream.shape[0]
    tok_start = lax.axis_index("sp") * tok_rows
    alpha = (2.0 * LAYERS) ** 0.25
    contract_rows = (((0,), (0,)), ((), ()))
    contract_cols = (((1,), (1,)), ((), ()))
    current = stream
    for layer_index in range(LAYERS):
        whole_in = lax.all_gather(in_weight[layer_index], "sp", axis=0, tiled=True)
        partial_value = lax.dot_general(
            whole_in, current, contract_cols, preferred_element_type=jnp.float32
        )
        hidden = lax.psum(partial_value.astype(jnp.bfloat16), "tp")
        pooled = pooled_windows(hidden, tok_start)
        grouped = pooled.reshape(GROUPS, GROUP_WIDTH, tok_rows)
        mixed = jnp.einsum(
            "gio,git->got", group_mix[layer_index], grouped, preferred_element_type=jnp.float32
        )
        gains = pool_gain[layer_index].reshape(GROUPS, GROUP_WIDTH, 1)
        scaled = (mixed * gains).astype(jnp.bfloat16).reshape(POOL, tok_rows)
        branch = lax.dot_general(
            scaled,
            lax.all_gather(out_weight[layer_index], "sp", axis=0, tiled=True),
            contract_rows,
            preferred_element_type=jnp.float32,
        )
        summed = alpha * current.astype(jnp.float32) + branch
        row_sum, row_squares = lax.psum(
            (jnp.sum(summed, axis=1), jnp.sum(summed * summed, axis=1)), "tp"
        )
        row_mean = row_sum / D
        row_var = row_squares / D - row_mean * row_mean
        normed = (summed - row_mean[:, None]) * lax.rsqrt(row_var + epsilon)[:, None]
        current = (
            normed * norm_gain[layer_index][None, :] + norm_shift[layer_index][None, :]
        ).astype(jnp.bfloat16)
    return current


def solution(mesh):
    in_specs = (
        P(("grp", "sp"), "tp"),
        P(None, "sp", "tp"),
        P(None, "sp", "tp"),
        P(),
        P(),
        P(None, "tp"),
        P(None, "tp"),
    )
    out_specs = P(("grp", "sp"), "tp")
    return jax.shard_map(
        per_device, mesh=mesh, in_specs=in_specs, out_specs=out_specs, check_vma=False
    )
```

profile of v0, /device:TPU:0, one launch (start us, length us, event | category | flops | bytes accessed | tf_op | source)
XLA Modules:
  0.0 312.8 jit_solution(13905823871252964514)
XLA Ops:
  6.5 2.2 fusion.49
  8.8 0.0 all-gather.9.cloned.1.call-update
  8.8 0.0 copy-start.2
  8.8 0.0 all-reduce.5.cloned.1.call-start
  8.9 48.5 %all-gather.9.cloned.1.call-done = bf16[1,1024,1024]{2,1,0:T(8,128)(2,1)} async-done(((bf16[1,256,1024]{2,1,0:T(8,128)(2,1)}), bf16[1,1024,1024]{2,1,0:T(8,128)(2,1)}) %all-gather.9.cloned.1.call-update) | async-done | bytes 2097168 | tf_op jit(solution)/shard_map/all_gather | solution.py:49
  57.3 5.0 %fusion.22 = bf16[1024,768]{1,0:T(8,128)(2,1)} fusion(bf16[768,1024]{1,0:T(8,128)(2,1)} %param.7, bf16[1,1024,1024]{2,1,0:T(8,128)(2,1)} %all-gather.9.cloned.1.call-done), kind=kOutput, calls=%fused_computation.40 | convolution fusion | flops 1611399168 | bytes 5242880 | tf_op jit(solution)/shard_map/dot_general | solution.py:50
  62.4 0.0 all-reduce.5.cloned.1.call-update
  62.4 0.0 all-gather.11.cloned.1.call-start
  62.4 1.1 fusion.48
  63.5 0.0 all-gather.11.cloned.1.call-update
  63.5 0.0 all-gather.13.cloned.1.call-start
  63.6 0.5 all-gather.13.cloned.1.call-update
  64.1 0.0 all-reduce.7.cloned.1.call-start
  64.3 0.0 copy-done.5
  64.3 39.9 %all-reduce.5.cloned.1.call-done = bf16[1024,768]{1,0:T(8,128)(2,1)} async-done(((bf16[1024,768]{1,0:T(8,128)(2,1)}), bf16[1024,768]{1,0:T(8,128)(2,1)}) %all-reduce.5.cloned.1.call-update) | async-done | bytes 1572880 | tf_op jit(solution)/shard_map/psum | solution.py:53
  104.2 1.1 slice.138
  105.3 3.4 %collective-permute-start = (bf16[1024,15]{1,0:T(8,128)(2,1)S(1)}, bf16[1024,15]{1,0:T(8,128)(2,1)S(1)}, u32[]{:S(2)}, u32[]{:S(2)}) collective-permute-start(bf16[1024,15]{1,0:T(8,128)(2,1)S(1)} %slice.138), channel_id=1, source_target_pairs={{0,4},{4,8},{8,12},{1,5},{5,9},{9,13},{2,6},{6,10},{10,14},{3,7},{... | collective-permute-start | bytes 92168 | tf_op jit(solution)/shard_map/ppermute | solution.py:17
  108.7 5.4 %collective-permute-done = bf16[1024,15]{1,0:T(8,128)(2,1)S(1)} collective-permute-done((bf16[1024,15]{1,0:T(8,128)(2,1)S(1)}, bf16[1024,15]{1,0:T(8,128)(2,1)S(1)}, u32[]{:S(2)}, u32[]{:S(2)}) %collective-permute-start) | collective-permute-done | bytes 30752 | tf_op jit(solution)/shard_map/ppermute | solution.py:17
  114.1 2.3 maximum_convert_fusion
  116.4 1.0 slice_add_fusion.5
  117.4 1.0 slice_add_fusion.4
  118.5 1.0 slice_add_fusion.3
  119.5 0.4 copy-done
  119.9 4.1 %fusion.1 = bf16[1024,768]{1,0:T(8,128)(2,1)S(1)} fusion(f32[1024,782]{1,0:T(8,128)S(1)} %slice_add_fusion.5, f32[1024,780]{1,0:T(8,128)S(1)} %slice_add_fusion.4, f32[1024,776]{1,0:T(8,128)S(1)} %slice_add_fusion.3, bf16[1024,768]{1,0:T(8,128)(2,1)S(1)} %copy-done, f32[1024]{0:T(1024)S(1)} %fusion.44, f32[768]{0:T(1024)S(1)} %add_convert_fusion.2, ...), kind=kLoop, calls=%fused_computation.9 | loop fusion | flops 7864320 | bytes 15739904 | tf_op jit(solution)/shard_map/convert_element_type | solution.py:38
  124.0 0.6 multiply_convert_fusion.1
  124.7 26.8 %all-gather.11.cloned.1.call-done = bf16[1,1024,1024]{2,1,0:T(8,128)(2,1)} async-done(((bf16[1,256,1024]{2,1,0:T(8,128)(2,1)}), bf16[1,1024,1024]{2,1,0:T(8,128)(2,1)}) %all-gather.11.cloned.1.call-update) | async-done | bytes 2097168 | tf_op jit(solution)/shard_map/all_gather | solution.py:63
  151.5 5.8 %fusion.47 = (f32[768]{0:T(1024)S(1)}, f32[768]{0:T(1024)S(1)}, f32[768,1024]{1,0:T(8,128)}) fusion(bf16[1024,768]{1,0:T(8,128)(2,1)S(1)} %bitcast.56, bf16[1,1024,1024]{2,1,0:T(8,128)(2,1)} %all-gather.11.cloned.1.call-done, bf16[768,1024]{1,0:T(8,128)(2,1)} %param.7), kind=kOutput, calls=%fused_computation.70 | convolution fusion | flops 1615329792 | bytes 8394752 | tf_op jit(solution)/shard_map/dot_general | solution.py:61
  157.3 6.5 %all-reduce.1 = (f32[768]{0:T(1024)S(1)}, f32[768]{0:T(1024)S(1)}) all-reduce(f32[768]{0:T(1024)S(1)} %get-tuple-element.8, f32[768]{0:T(1024)S(1)} %get-tuple-element.7), channel_id=1, replica_groups=mesh['grp'=2,'sp'=4,'tp'=4] {'tp'}, use_global_device_ids=true, to_apply=%region_4.5 | all-reduce | flops 1536 | bytes 12288 | tf_op jit(solution)/shard_map/psum | solution.py:68
  163.8 33.6 %all-gather.13.cloned.1.call-done = bf16[1,1024,1024]{2,1,0:T(8,128)(2,1)} async-done(((bf16[1,256,1024]{2,1,0:T(8,128)(2,1)}), bf16[1,1024,1024]{2,1,0:T(8,128)(2,1)}) %all-gather.13.cloned.1.call-update) | async-done | bytes 2097168 | tf_op jit(solution)/shard_map/all_gather | solution.py:49
  197.4 5.6 %fusion.28 = bf16[1024,768]{1,0:T(8,128)(2,1)} fusion(bf16[1,1024,1024]{2,1,0:T(8,128)(2,1)} %all-gather.13.cloned.1.call-done, f32[768,1024]{1,0:T(8,128)} %get-tuple-element.27, f32[1024]{0:T(1024)S(1)} %bitcast.61, f32[1024]{0:T(1024)S(1)} %bitcast.59, f32[768]{0:T(1024)S(1)} %get-tuple-element.26, f32[768]{0:T(1024)S(1)} %get-tuple-element.25), kind=kOutput, calls=%fused_computation.42 | convolution fusion | flops 1615331328 | bytes 6830080 | tf_op jit(solution)/shard_map/dot_general | solution.py:50
  203.1 0.0 all-reduce.7.cloned.1.call-update
  203.1 0.0 all-gather.15.cloned.1.call-start
  203.1 0.5 all-gather.15.cloned.1.call-update
  203.7 41.2 %all-reduce.7.cloned.1.call-done = bf16[1024,768]{1,0:T(8,128)(2,1)} async-done(((bf16[1024,768]{1,0:T(8,128)(2,1)}), bf16[1024,768]{1,0:T(8,128)(2,1)}) %all-reduce.7.cloned.1.call-update) | async-done | bytes 1572880 | tf_op jit(solution)/shard_map/psum | solution.py:53
  244.9 1.1 slice.149
  246.0 3.6 %collective-permute-start.1 = (bf16[1024,15]{1,0:T(8,128)(2,1)S(1)}, bf16[1024,15]{1,0:T(8,128)(2,1)S(1)}, u32[]{:S(2)}, u32[]{:S(2)}) collective-permute-start(bf16[1024,15]{1,0:T(8,128)(2,1)S(1)} %slice.149), channel_id=1, source_target_pairs={{0,4},{4,8},{8,12},{1,5},{5,9},{9,13},{2,6},{6,10},{10,14},{3,7},{... | collective-permute-start | bytes 92168 | tf_op jit(solution)/shard_map/ppermute | solution.py:17
  249.6 5.5 %collective-permute-done.1 = bf16[1024,15]{1,0:T(8,128)(2,1)S(1)} collective-permute-done((bf16[1024,15]{1,0:T(8,128)(2,1)S(1)}, bf16[1024,15]{1,0:T(8,128)(2,1)S(1)}, u32[]{:S(2)}, u32[]{:S(2)}) %collective-permute-start.1) | collective-permute-done | bytes 30752 | tf_op jit(solution)/shard_map/ppermute | solution.py:17
  255.2 2.2 maximum_convert_fusion.1
  257.4 1.0 slice_add_fusion.2
  258.4 1.0 slice_add_fusion.1
  259.4 1.0 slice_add_fusion
  260.5 0.4 copy-done.1
  260.9 4.1 %fusion.3 = bf16[1024,768]{1,0:T(8,128)(2,1)S(1)} fusion(f32[1024,782]{1,0:T(8,128)S(1)} %slice_add_fusion.2, f32[1024,780]{1,0:T(8,128)S(1)} %slice_add_fusion.1, f32[1024,776]{1,0:T(8,128)S(1)} %slice_add_fusion, bf16[1024,768]{1,0:T(8,128)(2,1)S(1)} %copy-done.1, f32[1024]{0:T(1024)S(1)} %fusion.44, f32[768]{0:T(1024)S(1)} %add_convert_fusion.2, ...), kind=kLoop, calls=%fused_computation.11 | loop fusion | flops 7864320 | bytes 15739904 | tf_op jit(solution)/shard_map/convert_element_type | solution.py:38
  265.0 1.8 multiply_convert_fusion
  266.8 25.3 %all-gather.15.cloned.1.call-done = bf16[1,1024,1024]{2,1,0:T(8,128)(2,1)} async-done(((bf16[1,256,1024]{2,1,0:T(8,128)(2,1)}), bf16[1,1024,1024]{2,1,0:T(8,128)(2,1)}) %all-gather.15.cloned.1.call-update) | async-done | bytes 2097168 | tf_op jit(solution)/shard_map/all_gather | solution.py:63
  292.1 5.6 %fusion.46 = (f32[768]{0:T(1024)S(1)}, f32[768]{0:T(1024)S(1)}, f32[768,1024]{1,0:T(8,128)S(1)}) fusion(bf16[1024,768]{1,0:T(8,128)(2,1)} %bitcast.55, bf16[1,1024,1024]{2,1,0:T(8,128)(2,1)} %all-gather.15.cloned.1.call-done, f32[1024]{0:T(1024)S(1)} %bitcast.62, f32[1024]{0:T(1024)S(1)} %bitcast.60, f32[768]{0:T(1024)S(1)} %get-tuple-element.26, ...), kind=kOutput, calls=%fused_computation.69 | convolution fusion | flops 1619261952 | bytes 9981952 | tf_op jit(solution)/shard_map/dot_general | solution.py:61
  297.7 6.5 %all-reduce = (f32[768]{0:T(1024)S(1)}, f32[768]{0:T(1024)S(1)}) all-reduce(f32[768]{0:T(1024)S(1)} %get-tuple-element.6, f32[768]{0:T(1024)S(1)} %get-tuple-element.5), channel_id=1, replica_groups=mesh['grp'=2,'sp'=4,'tp'=4] {'tp'}, use_global_device_ids=true, to_apply=%region_9.10 | all-reduce | flops 1536 | bytes 12288 | tf_op jit(solution)/shard_map/psum | solution.py:68
  304.2 1.7 add_convert_fusion
  (22 shorter events, 0.1 us)
Async XLA Ops:
  6.5 50.8 %all-gather.9.cloned.1.call-start = ((), (), s32[]{:S(2)}) async-start(), calls=%async_computation.2 | async-start | bytes 2621440 | tf_op jit(solution)/shard_map/all_gather | solution.py:49
  8.8 53.6 %copy-start.2 = (bf16[2,256,1024]{2,1,0:T(8,128)(2,1)S(1)}, bf16[2,256,1024]{2,1,0:T(8,128)(2,1)}, u32[]{:S(2)}) copy-start(bf16[2,256,1024]{2,1,0:T(8,128)(2,1)} %param.9) | copy-start | bytes 3145732
  8.8 95.4 %all-reduce.5.cloned.1.call-start = ((), (), s32[]{:S(2)}) async-start(), calls=%async_computation | async-start | bytes 3145728 | tf_op jit(solution)/shard_map/psum | solution.py:53
  62.3 1.9 copy-start.4
  62.3 1.9 copy-start.5
  62.3 1.9 copy-start.6
  62.4 89.1 %all-gather.11.cloned.1.call-start = ((), (), s32[]{:S(2)}) async-start(), calls=%async_computation.3 | async-start | bytes 2621440 | tf_op jit(solution)/shard_map/all_gather | solution.py:63
  63.5 133.9 %all-gather.13.cloned.1.call-start = ((), (), s32[]{:S(2)}) async-start(), calls=%async_computation.4 | async-start | bytes 2621440 | tf_op jit(solution)/shard_map/all_gather | solution.py:49
  64.1 180.8 %all-reduce.7.cloned.1.call-start = ((), (), s32[]{:S(2)}) async-start(), calls=%async_computation.1 | async-start | bytes 3145728 | tf_op jit(solution)/shard_map/psum | solution.py:53
  105.3 8.8 %collective-permute-start = (bf16[1024,15]{1,0:T(8,128)(2,1)S(1)}, bf16[1024,15]{1,0:T(8,128)(2,1)S(1)}, u32[]{:S(2)}, u32[]{:S(2)}) collective-permute-start(bf16[1024,15]{1,0:T(8,128)(2,1)S(1)} %slice.138), channel_id=1, source_target_pairs={{0,4},{4,8},{8,12},{1,5},{5,9},{9,13},{2,6},{6,10},{10,14},{3,7},{... | collective-permute-start | bytes 92168 | tf_op jit(solution)/shard_map/ppermute | solution.py:17
  118.5 1.4 copy-start
  119.9 4.1 %copy-start.3 = (bf16[2,4,256,256]{3,2,1,0:T(8,128)(2,1)S(1)}, bf16[2,4,256,256]{3,2,1,0:T(8,128)(2,1)}, u32[]{:S(2)}) copy-start(bf16[2,4,256,256]{3,2,1,0:T(8,128)(2,1)} %param.10) | copy-start | bytes 3145732
  203.1 89.0 %all-gather.15.cloned.1.call-start = ((), (), s32[]{:S(2)}) async-start(), calls=%async_computation.5 | async-start | bytes 2621440 | tf_op jit(solution)/shard_map/all_gather | solution.py:63
  246.0 9.2 %collective-permute-start.1 = (bf16[1024,15]{1,0:T(8,128)(2,1)S(1)}, bf16[1024,15]{1,0:T(8,128)(2,1)S(1)}, u32[]{:S(2)}, u32[]{:S(2)}) collective-permute-start(bf16[1024,15]{1,0:T(8,128)(2,1)S(1)} %slice.149), channel_id=1, source_target_pairs={{0,4},{4,8},{8,12},{1,5},{5,9},{9,13},{2,6},{6,10},{10,14},{3,7},{... | collective-permute-start | bytes 92168 | tf_op jit(solution)/shard_map/ppermute | solution.py:17
  259.4 1.4 copy-start.1
Sparse Core Ops, SparseCore 0:
  8.9 48.3 all-gather.8
  62.5 41.6 all-reduce.4
  105.8 45.7 all-gather.10
  152.9 44.4 all-gather.12
  203.2 41.6 all-reduce.6
  246.3 45.7 all-gather.14
where the time goes:
time: 313 us
  waiting for transfers between devices  227 us (73%)
  matrix products  24.5 us (8%)
  other arithmetic  20.6 us (7%)
  between operations  13.7 us (4%)
  blocking collectives  13 us (4%)
  starting transfers between devices  7.2 us (2%)
  local copies, waits for them, and re-layouts  6.35 us (2%)
    all_gather x2, waiting for transfers between devices, per_device(): whole_in = lax.all_gather(in_weight[layer_index], 'sp', axis=0, tiled=True)  82.1 us
    psum x2, waiting for transfers between devices, per_device(): hidden = lax.psum(partial_value.astype(jnp.bfloat16), 'tp')  81.1 us
    all_gather x2, waiting for transfers between devices, per_device(): lax.all_gather(out_weight[layer_index], 'sp', axis=0, tiled=True)  52.2 us
    psum x2, blocking collectives, per_device(): lax.psum((jnp.sum(summed, axis=1), jnp.sum(summed * summed, axis=1)), 'tp')  13 us
    dot_general x2, matrix products, per_device(): lax.dot_general(scaled, lax.all_gather(out_weight[layer_index], 'sp', axi...  11.4 us
    ppermute x2, waiting for transfers between devices, passed_along(): return lax.ppermute(block, axis, route)  10.9 us
    dot_general x2, matrix products, per_device(): lax.dot_general(whole_in, current, contract_cols, preferred_element_type=...  10.6 us
    convert_element_type x2, other arithmetic, pooled_windows(): (window_sums / counts - hidden.astype(jnp.float32)).astype(jnp.bfloat16)  8.26 us
  transfers between devices with their start and end apart: 8, of which 8 were waited for; matrix products, arithmetic and copies ran while one was open for 10% of the time, Pallas kernels for 0%

commit v1 on v0

--- a/solution.py
+++ b/solution.py
@@ -46,7 +46,10 @@
     contract_cols = (((1,), (1,)), ((), ()))
     current = stream
     for layer_index in range(LAYERS):
-        whole_in = lax.all_gather(in_weight[layer_index], "sp", axis=0, tiled=True)
+        whole_in = jnp.concatenate(
+            lax.all_to_all(jnp.stack([in_weight[layer_index]] * lax.axis_size("sp")), "sp", 0, 0),
+            axis=0,
+        )
         partial_value = lax.dot_general(
             whole_in, current, contract_cols, preferred_element_type=jnp.float32
         )

time: 313 us -> 272 us (0.87)
  waiting for transfers between devices: 227 us -> 128 us
  blocking collectives: 13 us -> 66.5 us
  starting transfers between devices: 7.2 us -> 10.7 us
    all_gather x2 -> x0, waiting for transfers between devices: 82.1 us -> none  [per_device(): whole_in = lax.all_gather(in_weight[layer_index], 'sp', axis=0, tiled=True)]
    all_to_all x0 -> x1, blocking collectives: none -> 54.5 us  [per_device(): lax.all_to_all(jnp.stack([in_weight[layer_index]] * lax.axis_size('sp')),...]
    all_gather x2, waiting for transfers between devices: 52.2 us -> 0.01 us  [per_device(): lax.all_gather(out_weight[layer_index], 'sp', axis=0, tiled=True)]
    ppermute x2, waiting for transfers between devices: 10.9 us -> 31.6 us  [passed_along(): return lax.ppermute(block, axis, route)]
    psum x2, waiting for transfers between devices: 81.1 us -> 95.4 us  [per_device(): hidden = lax.psum(partial_value.astype(jnp.bfloat16), 'tp')]
    all_to_all x0 -> x1, starting transfers between devices: none -> 3.76 us  [per_device(): lax.all_to_all(jnp.stack([in_weight[layer_index]] * lax.axis_size('sp')),...]
  transfers between devices with their start and end apart: 8 -> 7, of which waited for: 8 -> 4; matrix products, arithmetic and copies ran while one was open for 10% -> 12% of each run, Pallas kernels for 0% -> 0%
where the time goes in v1:
time: 272 us; the launch traced here: 271 us
  waiting for transfers between devices  128 us (47%)
  blocking collectives  66.5 us (24%)
  matrix products  23.4 us (9%)
  other arithmetic  20.6 us (8%)
  between operations  15.1 us (6%)
  starting transfers between devices  10.7 us (4%)
  local copies, waits for them, and re-layouts  7.23 us (3%)
    psum x2, waiting for transfers between devices, per_device(): hidden = lax.psum(partial_value.astype(jnp.bfloat16), 'tp')  95.4 us
    all_to_all x1, blocking collectives, per_device(): lax.all_to_all(jnp.stack([in_weight[layer_index]] * lax.axis_size('sp')),...  54.5 us
    ppermute x2, waiting for transfers between devices, passed_along(): return lax.ppermute(block, axis, route)  31.6 us
    psum x2, blocking collectives, per_device(): lax.psum((jnp.sum(summed, axis=1), jnp.sum(summed * summed, axis=1)), 'tp')  12 us
    dot_general x2, matrix products, per_device(): lax.dot_general(scaled, lax.all_gather(out_weight[layer_index], 'sp', axi...  11.9 us
    convert_element_type x2, other arithmetic, pooled_windows(): (window_sums / counts - hidden.astype(jnp.float32)).astype(jnp.bfloat16)  8.29 us
    dot_general x2, matrix products, per_device(): lax.dot_general(whole_in, current, contract_cols, preferred_element_type=...  7.97 us
    ppermute x2, starting transfers between devices, passed_along(): return lax.ppermute(block, axis, route)  6.81 us
  transfers between devices with their start and end apart: 7, of which 4 were waited for; matrix products, arithmetic and copies ran while one was open for 12% of the time, Pallas kernels for 0%

profile of v1, /device:TPU:0, one launch (start us, length us, event | category | flops | bytes accessed | tf_op | source)
XLA Modules:
  0.0 271.2 jit_solution(13875615155138149304)
XLA Ops:
  7.4 0.0 all-reduce.5.cloned.1.call-start
  7.4 1.3 slice_bitcast_fusion.1
  8.6 0.0 copy-start.7
  8.7 0.3 stack.6
  8.9 54.5 %all_to_all.10 = bf16[4,256,1024]{2,1,0:T(8,128)(2,1)S(1)} all-to-all(bf16[4,256,1024]{2,1,0:T(8,128)(2,1)S(1)} %stack.6), channel_id=1, replica_groups=mesh['grp'=2,'sp'=4,'tp'=4] {'sp'}, dimensions={0} | all-to-all | bytes 4194304 | tf_op jit(solution)/shard_map/all_to_all | solution.py:50
  63.4 3.0 %convolution_convert_fusion.1 = bf16[1024,768]{1,0:T(8,128)(2,1)} fusion(bf16[1024,1024]{1,0:T(8,128)(2,1)S(1)} %bitcast.52, bf16[768,1024]{1,0:T(8,128)(2,1)S(1)} %copy-done.7), kind=kOutput, calls=%fused_computation.37 | convolution fusion | flops 1611399168 | bytes 5242880 | tf_op jit(solution)/shard_map/dot_general | solution.py:53
  66.4 0.0 all-reduce.5.cloned.1.call-update
  66.4 0.0 copy-start.2
  66.4 1.6 stack.7
  68.0 3.8 %all-to-all-start.1 = ((bf16[4,256,1024]{2,1,0:T(8,128)(2,1)}), bf16[4,256,1024]{2,1,0:T(8,128)(2,1)S(1)}, u32[]{:S(2)}, u32[]{:S(2)}) async-start(bf16[4,256,1024]{2,1,0:T(8,128)(2,1)} %stack.7), calls=%async_computation.1 | async-start | bytes 4194304 | tf_op jit(solution)/shard_map/all_to_all | solution.py:50
  71.8 0.0 all-gather.5.cloned.1.call-start
  71.9 0.0 copy-done.2
  71.9 1.1 fusion.36
  72.9 0.0 all-gather.5.cloned.1.call-update
  73.0 0.0 all-reduce.7.cloned.1.call-start
  73.1 0.0 copy-done.6
  73.1 35.5 %all-reduce.5.cloned.1.call-done = bf16[1024,768]{1,0:T(8,128)(2,1)} async-done(((bf16[1024,768]{1,0:T(8,128)(2,1)}), bf16[1024,768]{1,0:T(8,128)(2,1)}) %all-reduce.5.cloned.1.call-update) | async-done | bytes 1572880 | tf_op jit(solution)/shard_map/psum | solution.py:56
  108.6 1.1 slice.144
  109.7 3.4 %collective-permute-start = (bf16[1024,15]{1,0:T(8,128)(2,1)S(1)}, bf16[1024,15]{1,0:T(8,128)(2,1)S(1)}, u32[]{:S(2)}, u32[]{:S(2)}) collective-permute-start(bf16[1024,15]{1,0:T(8,128)(2,1)S(1)} %slice.144), channel_id=1, source_target_pairs={{0,4},{4,8},{8,12},{1,5},{5,9},{9,13},{2,6},{6,10},{10,14},{3,7},{... | collective-permute-start | bytes 92168 | tf_op jit(solution)/shard_map/ppermute | solution.py:17
  113.2 26.2 %collective-permute-done = bf16[1024,15]{1,0:T(8,128)(2,1)S(1)} collective-permute-done((bf16[1024,15]{1,0:T(8,128)(2,1)S(1)}, bf16[1024,15]{1,0:T(8,128)(2,1)S(1)}, u32[]{:S(2)}, u32[]{:S(2)}) %collective-permute-start) | collective-permute-done | bytes 30752 | tf_op jit(solution)/shard_map/ppermute | solution.py:17
  139.4 2.2 maximum_convert_fusion
  141.7 1.0 slice_add_fusion.5
  142.7 1.0 slice_add_fusion.4
  143.7 1.0 slice_add_fusion.3
  144.7 0.4 copy-done
  145.1 4.1 %fusion.1 = bf16[1024,768]{1,0:T(8,128)(2,1)S(1)} fusion(f32[1024,782]{1,0:T(8,128)S(1)} %slice_add_fusion.5, f32[1024,780]{1,0:T(8,128)S(1)} %slice_add_fusion.4, f32[1024,776]{1,0:T(8,128)S(1)} %slice_add_fusion.3, bf16[1024,768]{1,0:T(8,128)(2,1)S(1)} %copy-done, f32[1024]{0:T(1024)S(1)} %fusion.32, f32[768]{0:T(1024)S(1)} %add_convert_fusion.2, ...), kind=kLoop, calls=%fused_computation.9 | loop fusion | flops 7864320 | bytes 15739904 | tf_op jit(solution)/shard_map/convert_element_type | solution.py:38
  149.3 1.8 multiply_convert_fusion.1
  151.1 6.3 %fusion.35 = (f32[768]{0:T(1024)S(1)}, f32[768]{0:T(1024)S(1)}, f32[768,1024]{1,0:T(8,128)}) fusion(bf16[1024,768]{1,0:T(8,128)(2,1)} %bitcast.54, bf16[1,1024,1024]{2,1,0:T(8,128)(2,1)} %all-gather.5.cloned.1.call-done, bf16[768,1024]{1,0:T(8,128)(2,1)} %param.7), kind=kOutput, calls=%fused_computation.68 | convolution fusion | flops 1615329792 | bytes 8394752 | tf_op jit(solution)/shard_map/dot_general | solution.py:64
  157.3 5.9 %all-reduce.1 = (f32[768]{0:T(1024)S(1)}, f32[768]{0:T(1024)S(1)}) all-reduce(f32[768]{0:T(1024)S(1)} %get-tuple-element.8, f32[768]{0:T(1024)S(1)} %get-tuple-element.7), channel_id=1, replica_groups=mesh['grp'=2,'sp'=4,'tp'=4] {'tp'}, use_global_device_ids=true, to_apply=%region_4.5 | all-reduce | flops 1536 | bytes 12288 | tf_op jit(solution)/shard_map/psum | solution.py:71
  163.3 0.0 all-to-all-done.1
  163.3 5.0 %fusion.18 = bf16[1024,768]{1,0:T(8,128)(2,1)} fusion(bf16[1024,1024]{1,0:T(8,128)(2,1)S(1)} %bitcast.51, f32[768,1024]{1,0:T(8,128)} %get-tuple-element.27, f32[1024]{0:T(1024)S(1)} %bitcast.59, f32[1024]{0:T(1024)S(1)} %bitcast.57, f32[768]{0:T(1024)S(1)} %get-tuple-element.26, f32[768]{0:T(1024)S(1)} %get-tuple-element.25), kind=kOutput, calls=%fused_computation.38 | convolution fusion | flops 1615331328 | bytes 6830080 | tf_op jit(solution)/shard_map/dot_general | solution.py:53
  168.3 0.0 all-reduce.7.cloned.1.call-update
  168.3 0.0 all-gather.7.cloned.1.call-start
  168.3 0.5 all-gather.7.cloned.1.call-update
  168.9 59.9 %all-reduce.7.cloned.1.call-done = bf16[1024,768]{1,0:T(8,128)(2,1)} async-done(((bf16[1024,768]{1,0:T(8,128)(2,1)}), bf16[1024,768]{1,0:T(8,128)(2,1)}) %all-reduce.7.cloned.1.call-update) | async-done | bytes 1572880 | tf_op jit(solution)/shard_map/psum | solution.py:56
  228.8 1.1 slice.155
  229.9 3.4 %collective-permute-start.1 = (bf16[1024,15]{1,0:T(8,128)(2,1)S(1)}, bf16[1024,15]{1,0:T(8,128)(2,1)S(1)}, u32[]{:S(2)}, u32[]{:S(2)}) collective-permute-start(bf16[1024,15]{1,0:T(8,128)(2,1)S(1)} %slice.155), channel_id=1, source_target_pairs={{0,4},{4,8},{8,12},{1,5},{5,9},{9,13},{2,6},{6,10},{10,14},{3,7},{... | collective-permute-start | bytes 92168 | tf_op jit(solution)/shard_map/ppermute | solution.py:17
  233.3 5.4 %collective-permute-done.1 = bf16[1024,15]{1,0:T(8,128)(2,1)S(1)} collective-permute-done((bf16[1024,15]{1,0:T(8,128)(2,1)S(1)}, bf16[1024,15]{1,0:T(8,128)(2,1)S(1)}, u32[]{:S(2)}, u32[]{:S(2)}) %collective-permute-start.1) | collective-permute-done | bytes 30752 | tf_op jit(solution)/shard_map/ppermute | solution.py:17
  238.7 2.2 maximum_convert_fusion.1
  241.0 1.0 slice_add_fusion.2
  242.0 1.0 slice_add_fusion.1
  243.0 1.0 slice_add_fusion
  244.0 0.4 copy-done.1
  244.4 4.1 %fusion.3 = bf16[1024,768]{1,0:T(8,128)(2,1)S(1)} fusion(f32[1024,782]{1,0:T(8,128)S(1)} %slice_add_fusion.2, f32[1024,780]{1,0:T(8,128)S(1)} %slice_add_fusion.1, f32[1024,776]{1,0:T(8,128)S(1)} %slice_add_fusion, bf16[1024,768]{1,0:T(8,128)(2,1)S(1)} %copy-done.1, f32[1024]{0:T(1024)S(1)} %fusion.32, f32[768]{0:T(1024)S(1)} %add_convert_fusion.2, ...), kind=kLoop, calls=%fused_computation.11 | loop fusion | flops 7864320 | bytes 15739904 | tf_op jit(solution)/shard_map/convert_element_type | solution.py:38
  248.6 1.8 multiply_convert_fusion
  250.4 5.6 %fusion.34 = (f32[768]{0:T(1024)S(1)}, f32[768]{0:T(1024)S(1)}, f32[768,1024]{1,0:T(8,128)S(1)}) fusion(bf16[1024,768]{1,0:T(8,128)(2,1)} %bitcast.53, bf16[1,1024,1024]{2,1,0:T(8,128)(2,1)} %all-gather.7.cloned.1.call-done, f32[1024]{0:T(1024)S(1)} %bitcast.60, f32[1024]{0:T(1024)S(1)} %bitcast.58, f32[768]{0:T(1024)S(1)} %get-tuple-element.26, ...), kind=kOutput, calls=%fused_computation.67 | convolution fusion | flops 1619261952 | bytes 9981952 | tf_op jit(solution)/shard_map/dot_general | solution.py:64
  256.0 6.1 %all-reduce = (f32[768]{0:T(1024)S(1)}, f32[768]{0:T(1024)S(1)}) all-reduce(f32[768]{0:T(1024)S(1)} %get-tuple-element.6, f32[768]{0:T(1024)S(1)} %get-tuple-element.5), channel_id=1, replica_groups=mesh['grp'=2,'sp'=4,'tp'=4] {'tp'}, use_global_device_ids=true, to_apply=%region_9.10 | all-reduce | flops 1536 | bytes 12288 | tf_op jit(solution)/shard_map/psum | solution.py:71
  262.1 1.7 add_convert_fusion
  (23 shorter events, 0.1 us)
Async XLA Ops:
  7.4 101.3 %all-reduce.5.cloned.1.call-start = ((), (), s32[]{:S(2)}) async-start(), calls=%async_computation.2 | async-start | bytes 3145728 | tf_op jit(solution)/shard_map/psum | solution.py:56
  8.6 54.8 %copy-start.7 = (bf16[768,1024]{1,0:T(8,128)(2,1)S(1)}, bf16[768,1024]{1,0:T(8,128)(2,1)}, u32[]{:S(2)}) copy-start(bf16[768,1024]{1,0:T(8,128)(2,1)} %param.7) | copy-start | bytes 4718596
  66.4 5.5 %copy-start.2 = (bf16[2,256,1024]{2,1,0:T(8,128)(2,1)S(1)}, bf16[2,256,1024]{2,1,0:T(8,128)(2,1)}, u32[]{:S(2)}) copy-start(bf16[2,256,1024]{2,1,0:T(8,128)(2,1)} %param.9) | copy-start | bytes 3145732
  68.0 5.0 %copy-start.4 = (f32[2,1024]{1,0:T(2,128)S(1)}, f32[2,1024]{1,0:T(2,128)}, u32[]{:S(2)}) copy-start(f32[2,1024]{1,0:T(2,128)} %param.11) | copy-start | bytes 24580
  68.0 5.0 %copy-start.5 = (f32[2,1024]{1,0:T(2,128)S(1)}, f32[2,1024]{1,0:T(2,128)}, u32[]{:S(2)}) copy-start(f32[2,1024]{1,0:T(2,128)} %param.12) | copy-start | bytes 24580
  68.0 5.1 %copy-start.6 = (f32[2,1024]{1,0:T(2,128)S(1)}, f32[2,1024]{1,0:T(2,128)}, u32[]{:S(2)}) copy-start(f32[2,1024]{1,0:T(2,128)} %param.13) | copy-start | bytes 24580
  68.0 95.2 %all-to-all-start.1 = ((bf16[4,256,1024]{2,1,0:T(8,128)(2,1)}), bf16[4,256,1024]{2,1,0:T(8,128)(2,1)S(1)}, u32[]{:S(2)}, u32[]{:S(2)}) async-start(bf16[4,256,1024]{2,1,0:T(8,128)(2,1)} %stack.7), calls=%async_computation.1 | async-start | bytes 4194304 | tf_op jit(solution)/shard_map/all_to_all | solution.py:50
  71.8 79.2 %all-gather.5.cloned.1.call-start = ((), (), s32[]{:S(2)}) async-start(), calls=%async_computation.4 | async-start | bytes 2621440 | tf_op jit(solution)/shard_map/all_gather | solution.py:66
  73.0 155.9 %all-reduce.7.cloned.1.call-start = ((), (), s32[]{:S(2)}) async-start(), calls=%async_computation.3 | async-start | bytes 3145728 | tf_op jit(solution)/shard_map/psum | solution.py:56
  109.7 29.7 %collective-permute-start = (bf16[1024,15]{1,0:T(8,128)(2,1)S(1)}, bf16[1024,15]{1,0:T(8,128)(2,1)S(1)}, u32[]{:S(2)}, u32[]{:S(2)}) collective-permute-start(bf16[1024,15]{1,0:T(8,128)(2,1)S(1)} %slice.144), channel_id=1, source_target_pairs={{0,4},{4,8},{8,12},{1,5},{5,9},{9,13},{2,6},{6,10},{10,14},{3,7},{... | collective-permute-start | bytes 92168 | tf_op jit(solution)/shard_map/ppermute | solution.py:17
  143.7 1.4 copy-start
  145.1 4.2 %copy-start.3 = (bf16[2,4,256,256]{3,2,1,0:T(8,128)(2,1)S(1)}, bf16[2,4,256,256]{3,2,1,0:T(8,128)(2,1)}, u32[]{:S(2)}) copy-start(bf16[2,4,256,256]{3,2,1,0:T(8,128)(2,1)} %param.10) | copy-start | bytes 3145732
  168.3 82.1 %all-gather.7.cloned.1.call-start = ((), (), s32[]{:S(2)}) async-start(), calls=%async_computation.5 | async-start | bytes 2621440 | tf_op jit(solution)/shard_map/all_gather | solution.py:66
  229.9 8.8 %collective-permute-start.1 = (bf16[1024,15]{1,0:T(8,128)(2,1)S(1)}, bf16[1024,15]{1,0:T(8,128)(2,1)S(1)}, u32[]{:S(2)}, u32[]{:S(2)}) collective-permute-start(bf16[1024,15]{1,0:T(8,128)(2,1)S(1)} %slice.155), channel_id=1, source_target_pairs={{0,4},{4,8},{8,12},{1,5},{5,9},{9,13},{2,6},{6,10},{10,14},{3,7},{... | collective-permute-start | bytes 92168 | tf_op jit(solution)/shard_map/ppermute | solution.py:17
  243.0 1.4 copy-start.1
Sparse Core Ops, SparseCore 0:
  66.5 42.0 all-reduce.4
  168.4 60.3 all-reduce.6
Sparse Core Ops, SparseCore 1:
  73.9 75.9 all-gather.4
  170.3 63.0 all-gather.6
